TPU v7x, 32 devices: a whole 2x2x4 slice. The times are simulated.
32 devices in a mesh: tp: 8 (over z, x), dp: 4 (over y, core).
Axes of the slice: x: 2, y: 2, z: 4, core: 2. Of those that a mesh axis runs over, the one named last changes fastest.
Arguments:
- tokens: bfloat16 [112, 4096], P('tp', 'dp'), may hold values from -6 to 6
- w_query: bfloat16 [2, 4096, 4096], P(None, 'dp', 'tp'), may hold values from -0.09375 to 0.09375
- w_key: bfloat16 [2, 4096, 4096], P(None, 'dp', 'tp'), may hold values from -0.09375 to 0.09375
- w_value: bfloat16 [2, 4096, 4096], P(None, 'dp', 'tp'), may hold values from -0.09375 to 0.09375
- w_outgate: bfloat16 [2, 4096, 4096], P(None, 'dp', 'tp'), may hold values from -0.09375 to 0.09375
- w_ingate: bfloat16 [2, 4096, 32], P(None, 'dp'), may hold values from -0.09375 to 0.09375
- w_forget: bfloat16 [2, 4096, 32], P(None, 'dp'), may hold values from -0.09375 to 0.09375
- forget_bias: float32 [2, 32], P(None, 'tp'), may hold values from -2 to 3
- head_gain: float32 [2, 32, 128], P(None, 'tp'), may hold values from 0.1 to 1.9
- w_proj: bfloat16 [2, 4096, 4096], P(None, 'tp', 'dp'), may hold values from -0.09375 to 0.09375
- mem_matrix: float32 [2, 112, 32, 128, 128], P(None, 'dp', 'tp'), may hold values from -0.8 to 0.8
- mem_norm: float32 [2, 112, 32, 128], P(None, 'dp', 'tp'), may hold values from -1.2 to 1.2
- mem_max: float32 [2, 112, 32], P(None, 'dp', 'tp'), may hold values from -4 to 4
Outputs:
- result: bfloat16 [112, 4096], P('tp', 'dp')
- new_matrix: float32 [2, 112, 32, 128, 128], P(None, 'dp', 'tp')
- new_norm: float32 [2, 112, 32, 128], P(None, 'dp', 'tp')
- new_max: float32 [2, 112, 32], P(None, 'dp', 'tp')
All inputs are finite; a program needn't handle non-finite values.
Results may differ from a plain program's by a relative error of at most 0.017.
Values may be sent and summed in bfloat16 or wider, within the bound.
A program may use at most 128 MiB of HBM per device.

v0:
```python
import jax
import jax.numpy as jnp
from jax import lax
from jax.sharding import PartitionSpec as P

HEAD = 128


norm_eps = 1e-06
head_eps = 1e-05


def cell_update(queries, key_vecs, values, log_in, log_forget, matrix, normvec, maxval):
    max_next = jnp.maximum(log_forget + maxval, log_in)
    decays = jnp.exp(log_forget + maxval - max_next)
    weight_in = jnp.exp(log_in - max_next)
    matrix_new = (
        decays[..., None, None] * matrix
        + weight_in[..., None, None] * key_vecs[..., :, None] * values[..., None, :]
    )
    norm_new = decays[..., None] * normvec + weight_in[..., None] * key_vecs
    numerator = jnp.einsum("bhd,bhde->bhe", queries, matrix_new, precision=lax.Precision.HIGHEST)
    denominator = jnp.maximum(jnp.abs(jnp.sum(queries * norm_new, axis=-1)), 1.0)
    return (numerator / denominator[..., None], matrix_new, norm_new, max_next)


def head_norm(readout, gain, outgate):
    average = jnp.mean(readout, axis=-1, keepdims=True)
    variance = jnp.mean(jnp.square(readout - average), axis=-1, keepdims=True)
    normed = (readout - average) * lax.rsqrt(variance + head_eps) * gain
    return normed * jax.nn.sigmoid(outgate)


def mix_block(gathered, weights, states):
    w_query, w_key, w_value, w_outgate, w_ingate, w_forget, bias, gain, w_proj = weights
    matrix, normvec, maxval = states
    features = gathered.shape[1] * lax.axis_size("dp")
    squares = jnp.sum(jnp.square(gathered.astype(jnp.float32)), axis=1)
    heads_dev = bias.shape[0]
    head_start = lax.axis_index("tp") * heads_dev
    gate_in = lax.dynamic_slice_in_dim(w_ingate, head_start, heads_dev, 1)
    gate_forget = lax.dynamic_slice_in_dim(w_forget, head_start, heads_dev, 1)
    part_query = jnp.dot(gathered, w_query, preferred_element_type=jnp.float32)
    part_key = jnp.dot(gathered, w_key, preferred_element_type=jnp.float32)
    part_value = jnp.dot(gathered, w_value, preferred_element_type=jnp.float32)
    part_outgate = jnp.dot(gathered, w_outgate, preferred_element_type=jnp.float32)
    part_ingate = jnp.dot(gathered, gate_in, preferred_element_type=jnp.float32)
    part_forget = jnp.dot(gathered, gate_forget, preferred_element_type=jnp.float32)
    rows_dev = gathered.shape[0] // lax.axis_size("dp")
    totals = lax.psum(squares, "dp")
    own_sum = lax.dynamic_slice_in_dim(totals, lax.axis_index("dp") * rows_dev, rows_dev, 0)
    sum_query, sum_key, sum_value, sum_outgate, sum_ingate, sum_forget = (
        lax.psum_scatter(part_query, "dp", scatter_dimension=0, tiled=True),
        lax.psum_scatter(part_key, "dp", scatter_dimension=0, tiled=True),
        lax.psum_scatter(part_value, "dp", scatter_dimension=0, tiled=True),
        lax.psum_scatter(part_outgate, "dp", scatter_dimension=0, tiled=True),
        lax.psum_scatter(part_ingate, "dp", scatter_dimension=0, tiled=True),
        lax.psum_scatter(part_forget, "dp", scatter_dimension=0, tiled=True),
    )
    inv_scale = lax.rsqrt(own_sum / features + norm_eps)[:, None]
    head_shape = (rows_dev, heads_dev, HEAD)
    queries = (sum_query * inv_scale).reshape(head_shape)
    key_vecs = (sum_key * inv_scale * HEAD ** (-0.5)).reshape(head_shape)
    values = (sum_value * inv_scale).reshape(head_shape)
    outgate = (sum_outgate * inv_scale).reshape(head_shape)
    log_in = sum_ingate * inv_scale
    log_forget = jax.nn.log_sigmoid(sum_forget * inv_scale + bias[None, :])
    readout, matrix_new, norm_new, max_next = cell_update(
        queries, key_vecs, values, log_in, log_forget, matrix, normvec, maxval
    )
    hidden = head_norm(readout, gain[None], outgate).reshape(rows_dev, -1).astype(jnp.bfloat16)
    out_partial = jnp.dot(
        lax.all_gather(hidden, "dp", axis=0, tiled=True), w_proj, preferred_element_type=jnp.float32
    )
    return (out_partial, matrix_new, norm_new, max_next)


def on_device(
    tokens,
    w_query,
    w_key,
    w_value,
    w_outgate,
    w_ingate,
    w_forget,
    forget_bias,
    head_gain,
    w_proj,
    mem_matrix,
    mem_norm,
    mem_max,
):
    current = lax.all_gather(tokens, "tp", axis=0, tiled=True)
    matrix_list, norm_list, max_list = ([], [], [])
    block_total = w_query.shape[0]
    result = current
    for block_id in range(block_total):
        weights = (
            w_query[block_id],
            w_key[block_id],
            w_value[block_id],
            w_outgate[block_id],
            w_ingate[block_id],
            w_forget[block_id],
            forget_bias[block_id],
            head_gain[block_id],
            w_proj[block_id],
        )
        out_partial, matrix_out, norm_out, max_out = mix_block(
            current, weights, (mem_matrix[block_id], mem_norm[block_id], mem_max[block_id])
        )
        matrix_list.append(matrix_out)
        norm_list.append(norm_out)
        max_list.append(max_out)
        if block_id + 1 < block_total:
            current = lax.psum(out_partial, "tp").astype(jnp.bfloat16)
        else:
            result = lax.psum_scatter(
                out_partial.astype(jnp.bfloat16), "tp", scatter_dimension=0, tiled=True
            )
    return (result, jnp.stack(matrix_list), jnp.stack(norm_list), jnp.stack(max_list))


def solution(mesh):
    in_specs = (
        P("tp", "dp"),
        P(None, "dp", "tp"),
        P(None, "dp", "tp"),
        P(None, "dp", "tp"),
        P(None, "dp", "tp"),
        P(None, "dp", None),
        P(None, "dp", None),
        P(None, "tp"),
        P(None, "tp", None),
        P(None, "tp", "dp"),
        P(None, "dp", "tp", None, None),
        P(None, "dp", "tp", None),
        P(None, "dp", "tp"),
    )
    out_specs = (
        P("tp", "dp"),
        P(None, "dp", "tp", None, None),
        P(None, "dp", "tp", None),
        P(None, "dp", "tp"),
    )
    return jax.shard_map(
        on_device, mesh=mesh, in_specs=in_specs, out_specs=out_specs, check_vma=False
    )
```

profile of v0, /device:TPU:0, one launch (start us, length us, event | category | flops | bytes accessed | tf_op | source)
XLA Modules:
  0.0 243.8 jit_solution(15858441146114237513)
XLA Ops:
  0.7 32.9 %all-gather = bf16[8,14,1024]{2,1,0:T(8,128)(2,1)S(1)} all-gather(bf16[1,14,1024]{2,1,0:T(8,128)(2,1)} %bitcast.149), channel_id=1, replica_groups=mesh['tp'=8,'dp'=4] {'tp'}, dimensions={0}, use_global_device_ids=true | all-gather | bytes 258048 | tf_op jit(solution)/shard_map/all_gather | solution.py:93
  33.6 1.5 fusion.36
  35.2 1.5 fusion.38
  36.7 1.5 fusion.40
  38.2 2.4 fusion.42
  40.6 14.0 %fusion.93 = (f32[32,512]{1,0:T(8,128)S(1)}, f32[32,512]{1,0:T(8,128)S(1)}, f32[32,512]{1,0:T(8,128)S(1)}, f32[32,512]{1,0:T(8,128)S(1)}) fusion(f32[112,512]{1,0:T(8,128)S(1)} %fusion.36, f32[112,512]{1,0:T(8,128)} %fusion.42, f32[112,512]{1,0:T(8,128)S(1)} %fusion.38, f32[112,512]{1,0:T(8,128)S(1)} %fusion.40), kind=kCustom, calls=%all-reduce-scatter.10 | all-reduce-scatter fusion | flops 262145 | bytes 1180160
  54.6 1.3 collective-permute-start.1
  55.9 3.7 %collective-permute-start.2 = (f32[12,512]{1,0:T(8,128)S(1)}, f32[12,512]{1,0:T(8,128)S(1)}, u32[]{:S(2)}, u32[]{:S(2)}) collective-permute-start(f32[12,512]{1,0:T(8,128)S(1)} %slice.98), channel_id=1, source_target_pairs={{0,1},{1,2},{2,3},{4,5},{5,6},{6,7},{8,9},{9,10},{10,11},{12,13},{... | collective-permute-start | bytes 73736
  59.6 1.9 collective-permute-start
  61.6 1.9 collective-permute-start.3
  66.1 1.3 fusion.100
  68.1 5.8 %all-reduce.23 = (f32[112]{0:T(128)S(1)}, f32[112,4]{0,1:T(4,128)S(1)}, f32[112,4]{0,1:T(4,128)S(1)}) all-reduce(f32[112]{0:T(128)S(1)} %multiply_reduce_fusion.1, f32[112,4]{0,1:T(4,128)S(1)} %convolution_bitcast_fusion.1, f32[112,4]{0,1:T(4,128)S(1)} %convolution_bitcast_fusion), channel_id=1, replica_groups=mesh['tp'=8,'dp'=4] {'dp'}, use_global_device_ids=true, to_apply=%region_2.0 | all-reduce | flops 1008 | bytes 8064 | tf_op jit(solution)/shard_map/psum | solution.py:50
  79.7 9.2 %fusion.13 = f32[28,4,1,128]{3,2,1,0:T(1,128)S(1)} fusion(f32[28,4,128,1]{2,3,1,0:T(1,128)S(1)} %bitcast.148, f32[2,28,4,128,128]{4,3,2,1,0:T(8,128)} %param.23, f32[28,4,128]{2,1,0:T(4,128)S(1)} %mul.321, f32[28,4,128]{2,1,0:T(4,128)S(1)} %get-tuple-element.37, f32[28,4]{1,0:T(8,128)S(1)} %copy.41), kind=kOutput, calls=%fused_computation.6 | convolution fusion | flops 27525120 | bytes 7569856 | tf_op jit(solution)/shard_map/bhd,bhde->bhe/dot_general | solution.py:22
  89.4 5.4 %all-gather.1 = bf16[4,28,512]{2,1,0:T(8,128)(2,1)S(1)} all-gather(bf16[1,28,512]{2,1,0:T(8,128)(2,1)S(1)} %reshape.136), channel_id=1, replica_groups=mesh['tp'=8,'dp'=4] {'dp'}, dimensions={0}, use_global_device_ids=true | all-gather | bytes 143360 | tf_op jit(solution)/shard_map/all_gather | solution.py:73
  95.2 43.0 %all-reduce.27 = bf16[112,1024]{1,0:T(8,128)(2,1)S(1)} all-reduce(f32[112,1024]{1,0:T(8,128)S(1)} %fusion.34), channel_id=1, replica_groups=mesh['tp'=8,'dp'=4] {'tp'}, use_global_device_ids=true, to_apply=%region_11.12 | all-reduce | flops 114688 | bytes 688128 | tf_op jit(solution)/shard_map/psum | solution.py:116
  138.4 1.5 fusion.28
  139.9 1.5 fusion.30
  141.4 1.5 fusion.32
  143.0 1.5 fusion.26
  144.8 5.7 %all-reduce.22 = (f32[112]{0:T(128)S(1)}, f32[112,4]{0,1:T(4,128)S(1)}, f32[112,4]{0,1:T(4,128)S(1)}) all-reduce(f32[112]{0:T(128)S(1)} %multiply_reduce_fusion, f32[112,4]{0,1:T(4,128)S(1)} %fusion.72, f32[112,4]{0,1:T(4,128)S(1)} %fusion.70), channel_id=1, replica_groups=mesh['tp'=8,'dp'=4] {'dp'}, use_global_device_ids=true, to_apply=%region_14.15 | all-reduce | flops 1008 | bytes 8064 | tf_op jit(solution)/shard_map/psum | solution.py:50
  150.9 14.6 %fusion.92 = (f32[32,512]{1,0:T(8,128)S(1)}, f32[32,512]{1,0:T(8,128)S(1)}, f32[32,512]{1,0:T(8,128)S(1)}, f32[32,512]{1,0:T(8,128)S(1)}) fusion(f32[112,512]{1,0:T(8,128)S(1)} %fusion.26, f32[112,512]{1,0:T(8,128)S(1)} %fusion.32, f32[112,512]{1,0:T(8,128)S(1)} %fusion.28, f32[112,512]{1,0:T(8,128)S(1)} %fusion.30), kind=kCustom, calls=%all-reduce-scatter.9 | all-reduce-scatter fusion | flops 262145 | bytes 1180160
  165.5 1.3 collective-permute-start.5
  166.8 3.8 %collective-permute-start.6 = (f32[12,512]{1,0:T(8,128)S(1)}, f32[12,512]{1,0:T(8,128)S(1)}, u32[]{:S(2)}, u32[]{:S(2)}) collective-permute-start(f32[12,512]{1,0:T(8,128)S(1)} %slice.102), channel_id=1, source_target_pairs={{0,1},{1,2},{2,3},{4,5},{5,6},{6,7},{8,9},{9,10},{10,11},{12,13},{... | collective-permute-start | bytes 73736
  170.6 1.9 collective-permute-start.4
  172.6 2.1 collective-permute-start.7
  176.8 14.1 %multiply_add_fusion.1 = (f32[1,28,4,128,128]{4,3,2,1,0:T(8,128)}, f32[1,28,4,128,128]{4,3,2,1,0:T(8,128)}) fusion(f32[2,28,4,128,128]{4,3,2,1,0:T(8,128)} %param.23, f32[28,4,128]{2,1,0:T(4,128)S(1)} %mul.321, f32[28,4,128]{2,1,0:T(4,128)S(1)} %get-tuple-element.37, f32[28,4]{1,0:T(8,128)S(1)} %copy.41, f32[28,4,128]{2,1,0:T(4,128)S(1)} %mul.347, ...), kind=kLoop, calls=%fused_computation.8 | loop fusion | flops 11010048 | bytes 29590400 | tf_op jit(solution)/shard_map/add | solution.py:18
  190.9 6.9 %fusion.10 = f32[28,4,1,128]{3,2,1,0:T(1,128)S(1)} fusion(f32[28,4,128,1]{2,3,1,0:T(1,128)S(1)} %bitcast.147, f32[2,28,4,128,128]{4,3,2,1,0:T(8,128)S(1)} %bitcast.144, f32[28,4,128]{2,1,0:T(4,128)S(1)} %mul.347, f32[28,4,128]{2,1,0:T(4,128)S(1)} %get-tuple-element.33, f32[28,4]{1,0:T(8,128)S(1)} %copy.44), kind=kOutput, calls=%fused_computation.3 | convolution fusion | flops 27525120 | bytes 7585792 | tf_op jit(solution)/shard_map/bhd,bhde->bhe/dot_general | solution.py:22
  198.4 5.4 %all-gather.2 = bf16[4,28,512]{2,1,0:T(8,128)(2,1)S(1)} all-gather(bf16[1,28,512]{2,1,0:T(8,128)(2,1)S(1)} %reshape.138), channel_id=1, replica_groups=mesh['tp'=8,'dp'=4] {'dp'}, dimensions={0}, use_global_device_ids=true | all-gather | bytes 143360 | tf_op jit(solution)/shard_map/all_gather | solution.py:73
  203.9 1.5 convolution_convert_fusion
  205.4 21.2 %fusion.8 = bf16[16,1024]{1,0:T(8,128)(2,1)S(1)} fusion(bf16[112,1024]{1,0:T(8,128)(2,1)S(1)} %convolution_convert_fusion), kind=kCustom, calls=%all-reduce-scatter.8 | all-reduce-scatter fusion | flops 131073 | bytes 262656
  226.6 2.1 collective-permute-start.8
  228.9 13.4 %pad_maximum_fusion = f32[2,28,4,128,128]{4,3,2,1,0:T(8,128)} fusion(f32[1,28,4,128,128]{4,3,2,1,0:T(8,128)} %get-tuple-element.39, f32[1,28,4,128,128]{4,3,2,1,0:T(8,128)} %get-tuple-element.38), kind=kLoop, calls=%fused_computation | loop fusion | flops 3670016 | bytes 29360128 | tf_op jit(solution)/shard_map/stack | solution.py:121
  (105 shorter events, 12.8 us)
Async XLA Ops:
  0.6 64.3 %copy-start.2 = (bf16[2,1024,32]{1,2,0:T(8,128)(2,1)S(1)}, bf16[2,1024,32]{1,2,0:T(8,128)(2,1)}, u32[]{:S(2)}) copy-start(bf16[2,1024,32]{1,2,0:T(8,128)(2,1)} %param.18) | copy-start | bytes 393220
  0.6 78.8 %copy-start.1 = (f32[2,28,4,128]{3,2,1,0:T(4,128)S(1)}, f32[2,28,4,128]{3,2,1,0:T(4,128)}, u32[]{:S(2)}) copy-start(f32[2,28,4,128]{3,2,1,0:T(4,128)} %param.24) | copy-start | bytes 344068
  38.2 56.7 %copy-start = (bf16[2,512,1024]{2,1,0:T(8,128)(2,1)S(1)}, bf16[2,512,1024]{2,1,0:T(8,128)(2,1)}, u32[]{:S(2)}) copy-start(bf16[2,512,1024]{2,1,0:T(8,128)(2,1)} %param.22) | copy-start | bytes 6291460
  54.6 23.8 %collective-permute-start.1 = (f32[12,512]{1,0:T(8,128)S(1)}, f32[12,512]{1,0:T(8,128)S(1)}, u32[]{:S(2)}, u32[]{:S(2)}) collective-permute-start(f32[12,512]{1,0:T(8,128)S(1)} %slice.97), channel_id=1, source_target_pairs={{0,1},{1,2},{2,3},{4,5},{5,6},{6,7},{8,9},{9,10},{10,11},{12,13},{... | collective-permute-start | bytes 73736
  55.9 22.6 %collective-permute-start.2 = (f32[12,512]{1,0:T(8,128)S(1)}, f32[12,512]{1,0:T(8,128)S(1)}, u32[]{:S(2)}, u32[]{:S(2)}) collective-permute-start(f32[12,512]{1,0:T(8,128)S(1)} %slice.98), channel_id=1, source_target_pairs={{0,1},{1,2},{2,3},{4,5},{5,6},{6,7},{8,9},{9,10},{10,11},{12,13},{... | collective-permute-start | bytes 73736
  59.6 19.2 %collective-permute-start = (f32[12,512]{1,0:T(8,128)S(1)}, f32[12,512]{1,0:T(8,128)S(1)}, u32[]{:S(2)}, u32[]{:S(2)}) collective-permute-start(f32[12,512]{1,0:T(8,128)S(1)} %slice.96), channel_id=1, source_target_pairs={{0,1},{1,2},{2,3},{4,5},{5,6},{6,7},{8,9},{9,10},{10,11},{12,13},{... | collective-permute-start | bytes 73736
  61.6 17.4 %collective-permute-start.3 = (f32[12,512]{1,0:T(8,128)S(1)}, f32[12,512]{1,0:T(8,128)S(1)}, u32[]{:S(2)}, u32[]{:S(2)}) collective-permute-start(f32[12,512]{1,0:T(8,128)S(1)} %slice.99), channel_id=1, source_target_pairs={{0,1},{1,2},{2,3},{4,5},{5,6},{6,7},{8,9},{9,10},{10,11},{12,13},{... | collective-permute-start | bytes 73736
  79.7 71.0 %copy-start.3 = (f32[2,28,4]{1,2,0:T(4,128)S(1)}, f32[2,28,4]{1,2,0:T(4,128)}, u32[]{:S(2)}) copy-start(f32[2,28,4]{1,2,0:T(4,128)} %param.25) | copy-start | bytes 2692
  79.7 71.0 %copy-start.4 = (f32[4]{0:T(128)S(1)}, f32[4]{0:T(128)}, u32[]{:S(2)}) copy-start(f32[4]{0:T(128)} %get-tuple-element.52) | copy-start | bytes 52
  165.5 10.0 %collective-permute-start.5 = (f32[12,512]{1,0:T(8,128)S(1)}, f32[12,512]{1,0:T(8,128)S(1)}, u32[]{:S(2)}, u32[]{:S(2)}) collective-permute-start(f32[12,512]{1,0:T(8,128)S(1)} %slice.101), channel_id=1, source_target_pairs={{0,1},{1,2},{2,3},{4,5},{5,6},{6,7},{8,9},{9,10},{10,11},{12,13},{... | collective-permute-start | bytes 73736
  166.8 8.9 %collective-permute-start.6 = (f32[12,512]{1,0:T(8,128)S(1)}, f32[12,512]{1,0:T(8,128)S(1)}, u32[]{:S(2)}, u32[]{:S(2)}) collective-permute-start(f32[12,512]{1,0:T(8,128)S(1)} %slice.102), channel_id=1, source_target_pairs={{0,1},{1,2},{2,3},{4,5},{5,6},{6,7},{8,9},{9,10},{10,11},{12,13},{... | collective-permute-start | bytes 73736
  170.6 5.2 %collective-permute-start.4 = (f32[12,512]{1,0:T(8,128)S(1)}, f32[12,512]{1,0:T(8,128)S(1)}, u32[]{:S(2)}, u32[]{:S(2)}) collective-permute-start(f32[12,512]{1,0:T(8,128)S(1)} %slice.100), channel_id=1, source_target_pairs={{0,1},{1,2},{2,3},{4,5},{5,6},{6,7},{8,9},{9,10},{10,11},{12,13},{... | collective-permute-start | bytes 73736
  172.6 3.5 %collective-permute-start.7 = (f32[12,512]{1,0:T(8,128)S(1)}, f32[12,512]{1,0:T(8,128)S(1)}, u32[]{:S(2)}, u32[]{:S(2)}) collective-permute-start(f32[12,512]{1,0:T(8,128)S(1)} %slice.103), channel_id=1, source_target_pairs={{0,1},{1,2},{2,3},{4,5},{5,6},{6,7},{8,9},{9,10},{10,11},{12,13},{... | collective-permute-start | bytes 73736
  176.5 14.4 %slice-start = ((s8[14680064]{0:T(1024)(128)(4,1)}), s8[2097152]{0:T(1024)(128)(4,1)S(1)}, s32[]{:S(2)}) async-start(s8[14680064]{0:T(1024)(128)(4,1)} %bitcast.143), calls=%async_computation | async-start | bytes 4194304
  176.8 14.1 %slice-start.1 = ((s8[14680064]{0:T(1024)(128)(4,1)}), s8[4194304]{0:T(1024)(128)(4,1)S(1)}, s32[]{:S(2)}) async-start(s8[14680064]{0:T(1024)(128)(4,1)} %bitcast.143), calls=%async_computation.1 | async-start | bytes 8388608
  176.8 14.1 %slice-start.2 = ((s8[14680064]{0:T(1024)(128)(4,1)}), s8[4194304]{0:T(1024)(128)(4,1)S(1)}, s32[]{:S(2)}) async-start(s8[14680064]{0:T(1024)(128)(4,1)} %bitcast.143), calls=%async_computation.2 | async-start | bytes 8388608
  176.8 14.1 %slice-start.3 = ((s8[14680064]{0:T(1024)(128)(4,1)}), s8[4194304]{0:T(1024)(128)(4,1)S(1)}, s32[]{:S(2)}) async-start(s8[14680064]{0:T(1024)(128)(4,1)} %bitcast.143), calls=%async_computation.3 | async-start | bytes 8388608
  226.6 16.3 %collective-permute-start.8 = (bf16[14,1024]{1,0:T(8,128)(2,1)S(1)}, bf16[14,1024]{1,0:T(8,128)(2,1)S(1)}, u32[]{:S(2)}, u32[]{:S(2)}) collective-permute-start(bf16[14,1024]{1,0:T(8,128)(2,1)S(1)} %slice.104), channel_id=1, source_target_pairs={{0,4},{4,8},{8,12},{12,16},{16,20},{20,24},{24,28},{1,5},{5,9},{9,... | collective-permute-start | bytes 86024
where the time goes:
time: 245 us; the launch traced here: 244 us
  blocking collectives  148 us (60%)
  other arithmetic  31.9 us (13%)
  matrix products  31.7 us (13%)
  starting transfers between devices  20 us (8%)
  local copies, waits for them, and re-layouts  8.64 us (4%)
  between operations  3.34 us (1%)
    unnamed x3, blocking collectives  49.8 us
    psum x1, blocking collectives, on_device(): current = lax.psum(out_partial, 'tp').astype(jnp.bfloat16)  43 us
    all_gather x1, blocking collectives, on_device(): current = lax.all_gather(tokens, 'tp', axis=0, tiled=True)  32.9 us
    unnamed x9, starting transfers between devices  20 us
    dot_general x2, matrix products, cell_update(): jnp.einsum('bhd,bhde->bhe', queries, matrix_new, precision=lax.Precision....  16.1 us
    add x1, other arithmetic, cell_update(): decays[..., None, None] * matrix  14.1 us
    another operation x1, other arithmetic, on_device(): jnp.stack(matrix_list)  13.4 us
    psum x2, blocking collectives, mix_block(): totals = lax.psum(squares, 'dp')  11.6 us
  transfers between devices with their start and end apart: 9, of which 0 were waited for; matrix products, arithmetic and copies ran while one was open for 10% of the time, Pallas kernels for 0%

commit v1 on v0

v1 whole, which is shorter than its diff:
```python
import functools

import jax
import jax.numpy as jnp
from jax import lax
from jax.experimental import pallas as pl
from jax.experimental.pallas import tpu as pltpu
from jax.sharding import PartitionSpec as P

HEAD = 128
norm_eps = 1e-06
head_eps = 1e-05
MESH = pl.DeviceIdType.MESH
F32 = jnp.float32
BF16 = jnp.bfloat16
PART = F32
OUTP = F32
SPLIT = True


def chain_kernel(
    n_tp,
    n_dp,
    rows_tp,
    heads_all,
    tok_ref,
    wq_hbm,
    wk_hbm,
    wv_hbm,
    wo_hbm,
    wg_hbm,
    bias_ref,
    gain_ref,
    wp_hbm,
    mat_hbm,
    norm_ref,
    max_ref,
    res_ref,
    wkey_ref,
    val_ref,
    dec_ref,
    normo_ref,
    maxo_ref,
    w_vm,
    wg_vm,
    wp_vm,
    mat_vm,
    xbuf,
    psend,
    precv,
    gsend,
    grecv,
    hbuf,
    osend,
    orecv,
    q_scr,
    qm_scr,
    w_sem,
    wg_sem,
    wp_sem,
    mat_sem,
    x_ssem,
    x_rsem,
    p_ssem,
    p_rsem,
    g_ssem,
    g_rsem,
    h_ssem,
    h_rsem,
    o_ssem,
    o_rsem,
):
    tp = lax.axis_index("tp")
    dp = lax.axis_index("dp")
    cells = w_vm.shape[0]
    rp, feats = tok_ref.shape
    cols = w_vm.shape[3]
    heads = cols // HEAD
    rd = hbuf.shape[2]
    rows = n_tp * rp

    def load(src, dst, sem):
        return pltpu.make_async_copy(src, dst, sem)

    def loads(b):
        out = [load(wg_hbm.at[b], wg_vm.at[b], wg_sem.at[b])]
        for j, w in enumerate((wq_hbm, wk_hbm, wv_hbm, wo_hbm)):
            out.append(load(w.at[b], w_vm.at[b, j], w_sem.at[b, j]))
        out.append(load(mat_hbm.at[b], mat_vm.at[b], mat_sem.at[b]))
        out.append(load(wp_hbm.at[b], wp_vm.at[b], wp_sem.at[b]))
        return out

    for c in loads(0):
        c.start()

    barrier = pltpu.get_barrier_semaphore()
    for i in range(1, n_tp):
        pl.semaphore_signal(
            barrier, inc=1, device_id={"tp": lax.rem(tp + i, n_tp)}, device_id_type=MESH
        )
    for i in range(1, n_dp):
        pl.semaphore_signal(
            barrier, inc=1, device_id={"dp": lax.rem(dp + i, n_dp)}, device_id_type=MESH
        )
    xbuf[0, tp] = tok_ref[...]
    qm_scr[...] = jnp.zeros_like(qm_scr)
    for b in range(1, cells):
        for c in loads(b):
            c.start()
    pl.semaphore_wait(barrier, n_tp + n_dp - 2)

    def push(src, dst, ssem, rsem, axis, peer):
        return pltpu.make_async_remote_copy(
            src_ref=src,
            dst_ref=dst,
            send_sem=ssem,
            recv_sem=rsem,
            device_id={axis: peer},
            device_id_type=MESH,
        )

    def peers(me, n):
        return [(i, lax.rem(me + i, n), lax.rem(me + n - i, n)) for i in range(1, n)]

    lane = lax.broadcasted_iota(jnp.int32, (HEAD, cols), 1) // HEAD
    gate = lax.broadcasted_iota(jnp.int32, (HEAD, cols), 0)
    pick_in = (gate == tp * heads + lane).astype(F32)
    pick_forget = (gate == heads_all + tp * heads + lane).astype(F32)
    pick_square = (gate == 2 * heads_all).astype(F32)

    def exact(a, b):
        return jnp.dot(a, b, precision=lax.Precision.HIGHEST, preferred_element_type=F32)

    def cell(b, carry):
        sends = []
        for i, to, frm in peers(tp, n_tp):
            c = push(
                xbuf.at[b, tp], xbuf.at[b, tp], x_ssem.at[b, i], x_rsem.at[b, i], "tp", to
            )
            c.start()
            sends.append(c)
        for i, to, frm in peers(tp, n_tp):
            push(
                xbuf.at[b, frm], xbuf.at[b, frm], x_ssem.at[b, i], x_rsem.at[b, i], "tp", to
            ).wait_recv()
        x = xbuf[b].reshape(rows, feats)
        load(wg_hbm.at[b], wg_vm.at[b], wg_sem.at[b]).wait()
        xf = x.astype(F32)
        square = jnp.sum(xf * xf, axis=1, keepdims=True)
        gates = jnp.dot(x, wg_vm[b], preferred_element_type=F32)
        spot = lax.broadcasted_iota(jnp.int32, gates.shape, 1)
        gates = jnp.where(spot == 2 * heads_all, square, gates)
        gsend[b] = gates.reshape(n_dp, rd, HEAD)
        for i, to, frm in peers(dp, n_dp):
            c = push(
                gsend.at[b, to], grecv.at[b, dp], g_ssem.at[b, i], g_rsem.at[b, i], "dp", to
            )
            c.start()
            sends.append(c)
        for j, w in enumerate((wq_hbm, wk_hbm, wv_hbm, wo_hbm)):
            load(w.at[b], w_vm.at[b, j], w_sem.at[b, j]).wait()
            part = jnp.dot(x, w_vm[b, j], preferred_element_type=F32)
            psend[b, j] = part.astype(PART).reshape(n_dp, rd, cols)
            for i, to, frm in peers(dp, n_dp):
                c = push(
                    psend.at[b, j, to],
                    precv.at[b, j, dp],
                    p_ssem.at[b, j, i],
                    p_rsem.at[b, j, i],
                    "dp",
                    to,
                )
                c.start()
                sends.append(c)
        for i, to, frm in peers(dp, n_dp):
            push(
                gsend.at[b, to], grecv.at[b, frm], g_ssem.at[b, i], g_rsem.at[b, i], "dp", to
            ).wait_recv()
        total = gsend[b, dp]
        for i, to, frm in peers(dp, n_dp):
            total = total + grecv[b, frm]
        squares = exact(total, pick_square)
        inv = lax.rsqrt(squares / (feats * n_dp) + norm_eps)
        log_in = exact(total, pick_in) * inv
        raw = exact(total, pick_forget) * inv + bias_ref[b]
        log_forget = jnp.minimum(raw, 0.0) - jnp.log1p(jnp.exp(-jnp.abs(raw)))
        held = log_forget + max_ref[b]
        max_next = jnp.maximum(held, log_in)
        decays = jnp.exp(held - max_next)
        weight_in = jnp.exp(log_in - max_next)

        def summed(j):
            for i, to, frm in peers(dp, n_dp):
                push(
                    psend.at[b, j, to],
                    precv.at[b, j, frm],
                    p_ssem.at[b, j, i],
                    p_rsem.at[b, j, i],
                    "dp",
                    to,
                ).wait_recv()
            acc = psend[b, j, dp].astype(F32)
            for i, to, frm in peers(dp, n_dp):
                acc = acc + precv[b, j, frm].astype(F32)
            return acc * inv

        query = summed(0)
        for h in range(heads):
            q_scr[h] = query[:, h * HEAD : (h + 1) * HEAD]
        load(mat_hbm.at[b], mat_vm.at[b], mat_sem.at[b]).wait()

        group = 7 if rows_tp % 7 == 0 else 1
        per = rows_tp // group

        first = lax.broadcasted_iota(jnp.int32, (16, HEAD), 0) == 0

        def read(step, carry):
            base = (step // per) * rp + lax.rem(step, per) * group
            for s in range(group):
                for h in range(heads):
                    row = q_scr[h, pl.ds(base + s, 1), :]
                    spread = jnp.broadcast_to(row, (16, HEAD))
                    high = spread.astype(BF16).astype(F32)
                    lhs = jnp.where(first, high, spread - high).astype(BF16)
                    m = mat_vm[b, step * group + s, h]
                    top = m.astype(BF16)
                    got = jnp.dot(lhs, top, preferred_element_type=F32)
                    if SPLIT:
                        rest = (m - top.astype(F32)).astype(BF16)
                        got = got + jnp.dot(lhs, rest, preferred_element_type=F32)
                    qm_scr[h, pl.ds(base + s, 1), :] = got[0:1] + got[1:2]
            return carry

        lax.fori_loop(0, mat_vm.shape[1] // group, read, 0)

        wkey = summed(1) * (HEAD**-0.5) * weight_in
        value = summed(2)
        outgate = summed(3)
        norm_new = decays * norm_ref[b] + wkey
        wkey_ref[b] = wkey
        val_ref[b] = value
        dec_ref[b] = decays
        normo_ref[b] = norm_new
        maxo_ref[b] = max_next
        for h in range(heads):
            at = slice(h * HEAD, (h + 1) * HEAD)
            qh = query[:, at]
            dot_n = jnp.sum(qh * norm_new[:, at], axis=1, keepdims=True)
            dot_k = jnp.sum(qh * wkey[:, at], axis=1, keepdims=True)
            top = decays[:, at] * qm_scr[h] + dot_k * value[:, at]
            readout = top / jnp.maximum(jnp.abs(dot_n), 1.0)
            average = jnp.mean(readout, axis=1, keepdims=True)
            away = readout - average
            variance = jnp.mean(away * away, axis=1, keepdims=True)
            normed = away * lax.rsqrt(variance + head_eps) * gain_ref[b][:, at]
            hidden = normed * jax.nn.sigmoid(outgate[:, at])
            hbuf[b, dp, :, at] = hidden.astype(BF16)
        for i, to, frm in peers(dp, n_dp):
            c = push(
                hbuf.at[b, dp], hbuf.at[b, dp], h_ssem.at[b, i], h_rsem.at[b, i], "dp", to
            )
            c.start()
            sends.append(c)
        load(wp_hbm.at[b], wp_vm.at[b], wp_sem.at[b]).wait()
        for i, to, frm in peers(dp, n_dp):
            push(
                hbuf.at[b, frm], hbuf.at[b, frm], h_ssem.at[b, i], h_rsem.at[b, i], "dp", to
            ).wait_recv()
        full = hbuf[b].reshape(rows, cols)
        out = jnp.dot(full, wp_vm[b], preferred_element_type=F32)
        osend[b] = out.astype(OUTP).reshape(n_tp, rp, feats)
        for i, to, frm in peers(tp, n_tp):
            c = push(
                osend.at[b, to], orecv.at[b, tp], o_ssem.at[b, i], o_rsem.at[b, i], "tp", to
            )
            c.start()
            sends.append(c)
        for i, to, frm in peers(tp, n_tp):
            push(
                osend.at[b, to], orecv.at[b, frm], o_ssem.at[b, i], o_rsem.at[b, i], "tp", to
            ).wait_recv()
        acc = osend[b, tp].astype(F32)
        for i, to, frm in peers(tp, n_tp):
            acc = acc + orecv[b, frm].astype(F32)
        xbuf[b + 1, tp] = acc.astype(BF16)
        for c in sends:
            c.wait_send()
        return carry

    lax.fori_loop(0, cells, cell, 0)
    res_ref[...] = xbuf[cells, tp]


def on_device(
    tokens,
    w_query,
    w_key,
    w_value,
    w_outgate,
    w_ingate,
    w_forget,
    forget_bias,
    head_gain,
    w_proj,
    mem_matrix,
    mem_norm,
    mem_max,
):
    n_tp, n_dp = lax.axis_size("tp"), lax.axis_size("dp")
    rows_tp, feats = tokens.shape
    rp = -(-rows_tp // 16) * 16
    cells, _, cols = w_query.shape
    seqs, heads = mem_max.shape[1:]
    blocks = seqs // rows_tp
    rd = blocks * rp
    heads_all = w_ingate.shape[2]
    more = rp - rows_tp

    def padded(a):
        a = a.reshape(cells, blocks, rows_tp, cols)
        return jnp.pad(a, ((0, 0), (0, 0), (0, more), (0, 0))).reshape(cells, rd, cols)

    def compact(a):
        a = a.reshape(cells, blocks, rp, heads, HEAD)[:, :, :rows_tp]
        return a.reshape(cells, seqs, heads, HEAD)

    def spread(a):
        return jnp.broadcast_to(a[..., None], a.shape + (HEAD,))

    toks = jnp.pad(tokens, ((0, more), (0, 0)))
    w_gate = jnp.concatenate([w_ingate, w_forget], axis=2)
    w_gate = jnp.pad(w_gate, ((0, 0), (0, 0), (0, HEAD - 2 * heads_all)))
    bias = spread(forget_bias).reshape(cells, 1, cols)
    gain = head_gain.reshape(cells, 1, cols)
    norm_in = padded(mem_norm)
    max_in = padded(spread(mem_max))

    vm = pl.BlockSpec(memory_space=pltpu.VMEM)
    hbm = pl.BlockSpec(memory_space=pl.ANY)
    dma = pltpu.SemaphoreType.DMA
    state = jax.ShapeDtypeStruct((cells, rd, cols), F32)
    result, wkey, value, decays, norm_new, max_new = pl.pallas_call(
        functools.partial(chain_kernel, n_tp, n_dp, rows_tp, heads_all),
        out_shape=(jax.ShapeDtypeStruct((rp, feats), BF16),) + (state,) * 5,
        in_specs=[vm, hbm, hbm, hbm, hbm, hbm, vm, vm, hbm, hbm, vm, vm],
        out_specs=(vm,) * 6,
        scratch_shapes=[
            pltpu.VMEM((cells, 4, feats, cols), BF16),
            pltpu.VMEM((cells, feats, HEAD), BF16),
            pltpu.VMEM((cells,) + w_proj.shape[1:], BF16),
            pltpu.VMEM(mem_matrix.shape, F32),
            pltpu.VMEM((cells + 1, n_tp, rp, feats), BF16),
            pltpu.VMEM((cells, 4, n_dp, rd, cols), PART),
            pltpu.VMEM((cells, 4, n_dp, rd, cols), PART),
            pltpu.VMEM((cells, n_dp, rd, HEAD), F32),
            pltpu.VMEM((cells, n_dp, rd, HEAD), F32),
            pltpu.VMEM((cells, n_dp, rd, cols), BF16),
            pltpu.VMEM((cells, n_tp, rp, feats), OUTP),
            pltpu.VMEM((cells, n_tp, rp, feats), OUTP),
            pltpu.VMEM((heads, rd, HEAD), F32),
            pltpu.VMEM((heads, rd, HEAD), F32),
            dma((cells, 4)),
            dma((cells,)),
            dma((cells,)),
            dma((cells,)),
            dma((cells, n_tp)),
            dma((cells, n_tp)),
            dma((cells, 4, n_dp)),
            dma((cells, 4, n_dp)),
            dma((cells, n_dp)),
            dma((cells, n_dp)),
            dma((cells, n_dp)),
            dma((cells, n_dp)),
            dma((cells, n_tp)),
            dma((cells, n_tp)),
        ],
        compiler_params=pltpu.CompilerParams(
            collective_id=0, has_side_effects=True, vmem_limit_bytes=56 * 2**20
        ),
    )(
        toks,
        w_query,
        w_key,
        w_value,
        w_outgate,
        w_gate,
        bias,
        gain,
        w_proj,
        mem_matrix,
        norm_in,
        max_in,
    )
    key_vecs = compact(wkey)
    values = compact(value)
    decay = compact(decays)[..., :1]
    matrix_new = decay[..., None] * mem_matrix + key_vecs[..., :, None] * values[..., None, :]
    return (result[:rows_tp], matrix_new, compact(norm_new), compact(max_new)[..., 0])


def solution(mesh):
    in_specs = (
        P("tp", "dp"),
        P(None, "dp", "tp"),
        P(None, "dp", "tp"),
        P(None, "dp", "tp"),
        P(None, "dp", "tp"),
        P(None, "dp", None),
        P(None, "dp", None),
        P(None, "tp"),
        P(None, "tp", None),
        P(None, "tp", "dp"),
        P(None, "dp", "tp", None, None),
        P(None, "dp", "tp", None),
        P(None, "dp", "tp"),
    )
    out_specs = (
        P("tp", "dp"),
        P(None, "dp", "tp", None, None),
        P(None, "dp", "tp", None),
        P(None, "dp", "tp"),
    )
    return jax.shard_map(
        on_device, mesh=mesh, in_specs=in_specs, out_specs=out_specs, check_vma=False
    )
```

time: 245 us -> 112 us (0.46)
  the two profiles are of different devices: /device:TPU:0 before, /device:TPU:31 now
where the time goes in v1:
time: 112 us
  Pallas kernels  82.6 us (74%)
  local copies, waits for them, and re-layouts  15.6 us (14%)
  other arithmetic  12.7 us (11%)
    pallas_call x1, Pallas kernels, on_device(): pl.pallas_call(functools.partial(chain_kernel, n_tp, n_dp, rows_tp, heads...  82.6 us
    add x1, other arithmetic, on_device(): decay[..., None] * mem_matrix  11.6 us
    reshape x5, local copies, waits for them, and re-layouts, compact(): a = a.reshape(cells, blocks, rp, heads, HEAD)[:, :, :rows_tp]  4.74 us
    unnamed x8, local copies, waits for them, and re-layouts  4.27 us

profile of v1, /device:TPU:31, one launch (start us, length us, event | category | flops | bytes accessed | tf_op | source)
XLA Modules:
  0.0 111.7 jit_solution(9263641931747389115)
XLA Ops:
  0.6 1.3 %broadcast_in_dim.4 = f32[2,4,128]{2,1,0:T(4,128)} broadcast(f32[2,4]{1,0:T(2,128)} %param.20), dimensions={0,1} | broadcast | bytes 4128 | tf_op jit(solution)/shard_map/broadcast_in_dim | solution.py:328
  2.0 0.8 copy.34
  2.8 1.4 %pad.15.tok_ref = bf16[16,1024]{1,0:T(8,128)(2,1)} pad(bf16[14,1024]{1,0:T(8,128)(2,1)} %param.13, bf16[]{:T(256)} %constant.3.clone.1), padding=0_2x0_0 | pad | bytes 61442 | tf_op jit(solution)/shard_map/jit(_pad)/pad | solution.py:330
  4.1 0.1 broadcast_in_dim.5
  4.3 0.1 reshape.59
  4.4 0.7 pad.18.clone
  5.1 0.9 reshape.69
  6.0 0.6 pad.17.clone
  6.6 1.2 %copy.30 = bf16[2,1024,32]{2,1,0:T(8,128)(2,1)S(1)} copy(bf16[2,1024,32]{1,2,0:T(8,128)(2,1)} %param.18) | data formatting | bytes 262144 | tf_op args[5]
  7.8 1.2 %copy.31 = bf16[2,1024,32]{2,1,0:T(8,128)(2,1)S(1)} copy(bf16[2,1024,32]{1,2,0:T(8,128)(2,1)} %param.19) | data formatting | bytes 262144 | tf_op args[6]
  9.0 1.2 %fusion.2.wg_hbm = bf16[2,1024,128]{2,1,0:T(8,128)(2,1)} fusion(bf16[2,1024,32]{2,1,0:T(8,128)(2,1)S(1)} %copy.31, bf16[2,1024,32]{2,1,0:T(8,128)(2,1)S(1)} %copy.30), kind=kLoop, calls=%fused_computation.4 | loop fusion | flops 1835008 | bytes 786432 | tf_op jit(solution)/shard_map/concatenate | solution.py:331
  10.2 82.6 %shard_map.156 = (bf16[16,1024]{1,0:T(8,128)(2,1)}, f32[2,32,512]{2,1,0:T(8,128)}, f32[2,32,512]{2,1,0:T(8,128)}, f32[2,32,512]{2,1,0:T(8,128)}, f32[2,32,512]{2,1,0:T(8,128)}, /*index=5*/f32[2,32,512]{2,1,0:T(8,128)}) custom-call(bf16[16,1024]{1,0:T(8,128)(2,1)} %pad.15.tok_ref, bf16[2,1024,512]{2,1,0:T(8,128)(2,1)} %wq_hbm.1, ...), custom_call_target="tpu_custom_call" | custom-call | tf_op jit(solution)/shard_map/pallas_call | solution.py:342
  92.8 0.9 reshape.61
  93.8 0.5 copy.39
  94.3 0.9 reshape.63
  95.2 0.9 reshape.64
  96.2 0.9 reshape.65
  97.1 0.7 slice.36
  97.8 0.9 reshape.67
  98.8 0.7 copy.37
  99.5 0.0 copy-start
  99.5 11.6 %multiply_add_fusion = f32[2,28,4,128,128]{4,3,2,1,0:T(8,128)} fusion(f32[2,28,4,128,128]{4,3,2,1,0:T(8,128)} %mat_hbm.1, f32[2,28,4,128]{3,2,1,0:T(4,128)S(1)} %bitcast.19, f32[2,28,4,128]{3,2,1,0:T(4,128)S(1)} %bitcast.18, f32[2,28,4]{2,1,0:T(8,128)S(1)} %bitcast.22), kind=kLoop, calls=%fused_computation | loop fusion | flops 11010048 | bytes 29590400 | tf_op jit(solution)/shard_map/add | solution.py:397
  111.1 0.0 copy-done
  111.1 0.6 copy.43
  (5 shorter events, 0.1 us)
Async XLA Ops:
  99.5 11.6 %copy-start = (bf16[16,1024]{1,0:T(8,128)(2,1)S(1)}, bf16[16,1024]{1,0:T(8,128)(2,1)}, u32[]{:S(2)}) copy-start(bf16[16,1024]{1,0:T(8,128)(2,1)} %get-tuple-element.10) | copy-start | bytes 98308

commit v2 on v1

--- a/solution.py
+++ b/solution.py
@@ -28,7 +28,8 @@
     wk_hbm,
     wv_hbm,
     wo_hbm,
-    wg_hbm,
+    wi_hbm,
+    wf_hbm,
     bias_ref,
     gain_ref,
     wp_hbm,
@@ -73,7 +74,7 @@
     tp = lax.axis_index("tp")
     dp = lax.axis_index("dp")
     cells = w_vm.shape[0]
-    rp, feats = tok_ref.shape
+    rp, feats = xbuf.shape[2:]
     cols = w_vm.shape[3]
     heads = cols // HEAD
     rd = hbuf.shape[2]
@@ -82,8 +83,15 @@
     def load(src, dst, sem):
         return pltpu.make_async_copy(src, dst, sem)
 
+    def gate_loads(b):
+        low, high = pl.ds(0, heads_all), pl.ds(heads_all, heads_all)
+        return [
+            load(wi_hbm.at[b], wg_vm.at[b, low], wg_sem.at[b, 0]),
+            load(wf_hbm.at[b], wg_vm.at[b, high], wg_sem.at[b, 1]),
+        ]
+
     def loads(b):
-        out = [load(wg_hbm.at[b], wg_vm.at[b], wg_sem.at[b])]
+        out = gate_loads(b)
         for j, w in enumerate((wq_hbm, wk_hbm, wv_hbm, wo_hbm)):
             out.append(load(w.at[b], w_vm.at[b, j], w_sem.at[b, j]))
         out.append(load(mat_hbm.at[b], mat_vm.at[b], mat_sem.at[b]))
@@ -102,7 +110,9 @@
         pl.semaphore_signal(
             barrier, inc=1, device_id={"dp": lax.rem(dp + i, n_dp)}, device_id_type=MESH
         )
-    xbuf[0, tp] = tok_ref[...]
+    xbuf[0, tp] = jnp.zeros((rp, feats), BF16)
+    xbuf[0, tp, :rows_tp] = tok_ref[...]
+    wg_vm[:, 2 * heads_all :] = jnp.zeros((cells, HEAD - 2 * heads_all, feats), BF16)
     qm_scr[...] = jnp.zeros_like(qm_scr)
     for b in range(1, cells):
         for c in loads(b):
@@ -144,10 +154,13 @@
                 xbuf.at[b, frm], xbuf.at[b, frm], x_ssem.at[b, i], x_rsem.at[b, i], "tp", to
             ).wait_recv()
         x = xbuf[b].reshape(rows, feats)
-        load(wg_hbm.at[b], wg_vm.at[b], wg_sem.at[b]).wait()
+        for c in gate_loads(b):
+            c.wait()
         xf = x.astype(F32)
         square = jnp.sum(xf * xf, axis=1, keepdims=True)
-        gates = jnp.dot(x, wg_vm[b], preferred_element_type=F32)
+        gates = lax.dot_general(
+            x, wg_vm[b], (((1,), (1,)), ((), ())), preferred_element_type=F32
+        )
         spot = lax.broadcasted_iota(jnp.int32, gates.shape, 1)
         gates = jnp.where(spot == 2 * heads_all, square, gates)
         gsend[b] = gates.reshape(n_dp, rd, HEAD)
@@ -327,9 +340,7 @@
     def spread(a):
         return jnp.broadcast_to(a[..., None], a.shape + (HEAD,))
 
-    toks = jnp.pad(tokens, ((0, more), (0, 0)))
-    w_gate = jnp.concatenate([w_ingate, w_forget], axis=2)
-    w_gate = jnp.pad(w_gate, ((0, 0), (0, 0), (0, HEAD - 2 * heads_all)))
+    w_in, w_fg = jnp.swapaxes(w_ingate, 1, 2), jnp.swapaxes(w_forget, 1, 2)
     bias = spread(forget_bias).reshape(cells, 1, cols)
     gain = head_gain.reshape(cells, 1, cols)
     norm_in = padded(mem_norm)
@@ -342,11 +353,11 @@
     result, wkey, value, decays, norm_new, max_new = pl.pallas_call(
         functools.partial(chain_kernel, n_tp, n_dp, rows_tp, heads_all),
         out_shape=(jax.ShapeDtypeStruct((rp, feats), BF16),) + (state,) * 5,
-        in_specs=[vm, hbm, hbm, hbm, hbm, hbm, vm, vm, hbm, hbm, vm, vm],
+        in_specs=[vm, hbm, hbm, hbm, hbm, hbm, hbm, vm, vm, hbm, hbm, vm, vm],
         out_specs=(vm,) * 6,
         scratch_shapes=[
             pltpu.VMEM((cells, 4, feats, cols), BF16),
-            pltpu.VMEM((cells, feats, HEAD), BF16),
+            pltpu.VMEM((cells, HEAD, feats), BF16),
             pltpu.VMEM((cells,) + w_proj.shape[1:], BF16),
             pltpu.VMEM(mem_matrix.shape, F32),
             pltpu.VMEM((cells + 1, n_tp, rp, feats), BF16),
@@ -360,7 +371,7 @@
             pltpu.VMEM((heads, rd, HEAD), F32),
             pltpu.VMEM((heads, rd, HEAD), F32),
             dma((cells, 4)),
-            dma((cells,)),
+            dma((cells, 2)),
             dma((cells,)),
             dma((cells,)),
             dma((cells, n_tp)),
@@ -378,12 +389,13 @@
             collective_id=0, has_side_effects=True, vmem_limit_bytes=56 * 2**20
         ),
     )(
-        toks,
+        tokens,
         w_query,
         w_key,
         w_value,
         w_outgate,
-        w_gate,
+        w_in,
+        w_fg,
         bias,
         gain,
         w_proj,

time: 112 us -> 107 us (0.955)
  local copies, waits for them, and re-layouts: 15.6 us -> 11.9 us
    unnamed x8 -> x6, local copies, waits for them, and re-layouts: 4.27 us -> 1.92 us
    pad x1 -> x0, local copies, waits for them, and re-layouts: 1.38 us -> none  [on_device(): toks = jnp.pad(tokens, ((0, more), (0, 0)))]
    concatenate x1 -> x0, other arithmetic: 1.16 us -> none  [on_device(): w_gate = jnp.concatenate([w_ingate, w_forget], axis=2)]
where the time goes in v2:
time: 107 us
  Pallas kernels  82.7 us (77%)
  local copies, waits for them, and re-layouts  11.9 us (11%)
  other arithmetic  11.6 us (11%)
    pallas_call x1, Pallas kernels, on_device(): pl.pallas_call(functools.partial(chain_kernel, n_tp, n_dp, rows_tp, heads...  82.7 us
    add x1, other arithmetic, on_device(): decay[..., None] * mem_matrix  11.6 us
    reshape x5, local copies, waits for them, and re-layouts, compact(): a = a.reshape(cells, blocks, rp, heads, HEAD)[:, :, :rows_tp]  4.74 us

profile of v2, /device:TPU:31, one launch (start us, length us, event | category | flops | bytes accessed | tf_op | source)
XLA Modules:
  0.0 106.8 jit_solution(11228127012830669726)
XLA Ops:
  0.6 1.3 %broadcast_in_dim.4 = f32[2,4,128]{2,1,0:T(4,128)} broadcast(f32[2,4]{1,0:T(2,128)} %param.20), dimensions={0,1} | broadcast | bytes 4128 | tf_op jit(solution)/shard_map/broadcast_in_dim | solution.py:341
  2.0 0.8 copy.28
  2.8 0.1 broadcast_in_dim.5
  2.9 0.1 reshape.59
  3.0 0.6 pad.8.clone
  3.7 0.9 reshape.69
  4.6 0.7 pad.7.clone
  5.3 82.7 %shard_map.156 = (bf16[16,1024]{1,0:T(8,128)(2,1)}, f32[2,32,512]{2,1,0:T(8,128)}, f32[2,32,512]{2,1,0:T(8,128)}, f32[2,32,512]{2,1,0:T(8,128)}, f32[2,32,512]{2,1,0:T(8,128)}, /*index=5*/f32[2,32,512]{2,1,0:T(8,128)}) custom-call(bf16[14,1024]{1,0:T(8,128)(2,1)} %tok_ref.1, bf16[2,1024,512]{2,1,0:T(8,128)(2,1)} %wq_hbm.1, bf16[2,1024,512]{2,1,0:T(8,128)(2,1)} %wk_hbm.1, ...), custom_call_target="tpu_custom_call" | custom-call | tf_op jit(solution)/shard_map/pallas_call | solution.py:353
  88.0 0.9 reshape.61
  88.9 0.5 copy.33
  89.4 0.9 reshape.63
  90.4 0.9 reshape.64
  91.3 0.9 reshape.65
  92.3 0.7 slice.36
  93.0 0.9 reshape.67
  93.9 0.7 copy.31
  94.6 0.0 copy-start
  94.6 11.6 %multiply_add_fusion = f32[2,28,4,128,128]{4,3,2,1,0:T(8,128)} fusion(f32[2,28,4,128,128]{4,3,2,1,0:T(8,128)} %mat_hbm.1, f32[2,28,4,128]{3,2,1,0:T(4,128)S(1)} %bitcast.21, f32[2,28,4,128]{3,2,1,0:T(4,128)S(1)} %bitcast.20, f32[2,28,4]{2,1,0:T(8,128)S(1)} %bitcast.26), kind=kLoop, calls=%fused_computation | loop fusion | flops 11010048 | bytes 29590400 | tf_op jit(solution)/shard_map/add | solution.py:409
  106.2 0.0 copy-done
  106.2 0.6 copy.37
  (5 shorter events, 0.1 us)
Async XLA Ops:
  94.6 11.6 %copy-start = (bf16[16,1024]{1,0:T(8,128)(2,1)S(1)}, bf16[16,1024]{1,0:T(8,128)(2,1)}, u32[]{:S(2)}) copy-start(bf16[16,1024]{1,0:T(8,128)(2,1)} %get-tuple-element.10) | copy-start | bytes 98308
